TPU v7x, 32 devices: a whole 2x2x4 slice. The times are simulated.
32 devices in a mesh: grp: 2 (over y), sp: 4 (over z), tp: 4 (over x, core).
Axes of the slice: x: 2, y: 2, z: 4, core: 2. Of those that a mesh axis runs over, the one named last changes fastest.
Arguments:
- queries: bfloat16 [1024, 512], P(('grp', 'sp'), 'tp'), parts along dimension 0, may hold values from -6 to 6
- key_rows: bfloat16 [1024, 512], P(('grp', 'sp'), 'tp'), parts along dimension 0, may hold values from -6 to 6
- value_rows: bfloat16 [1024, 512], P(('grp', 'sp'), 'tp'), parts along dimension 0, may hold values from -16 to 16
- key_bias: bfloat16 [8, 1024], P('tp', ('grp', 'sp')), parts along dimension 1, may hold values from -20 to 0
- residual: bfloat16 [1024, 2048], P(('grp', 'sp')), parts along dimension 0, may hold values from -6 to 6
- out_weight: bfloat16 [512, 2048], P('tp'), may hold values from -0.25 to 0.25
- norm_gain: bfloat16 [2048], replicated, may hold values from 0.099609375 to 1.8984375
- gate_weight: bfloat16 [2048, 3072], P('sp', 'tp'), may hold values from -0.125 to 0.125
- up_weight: bfloat16 [2048, 3072], P('sp', 'tp'), may hold values from -0.125 to 0.125
- down_weight: bfloat16 [3072, 2048], P('tp', 'sp'), may hold values from -0.109375 to 0.109375
Outputs:
- layer_out: bfloat16 [1024, 2048], P(('grp', 'sp')), parts along dimension 0
There are 2 independent parts, one for each index of `grp`. A program takes and returns all parts, laid end to end along the dimension named above; an argument that names none is the same for every part. Nothing has to cross between parts.
All inputs are finite; a program needn't handle non-finite values.
Results may differ from a plain program's by a relative error of at most 0.014.
Values may be sent and summed in bfloat16 or wider, within the bound.
A program may use at most 64 MiB of HBM per device.

v0:
```python
import jax
import jax.numpy as jnp
from jax import lax
from jax.sharding import PartitionSpec as P

norm_eps = 1e-05


def from_behind(value, axis, steps):
    count = lax.axis_size(axis)
    initial, last = (max(0, -steps), min(count, count - steps))
    return lax.ppermute(value, axis, [(source, source + steps) for source in range(initial, last)])


def stick_block(carry, query_heads, key_block, value_block, bias_block, query_pos, key_start):
    accum, kept_log = carry
    key_count = key_block.shape[0]
    head_count = query_heads.shape[1]
    key_heads = key_block.reshape(key_count, head_count, -1)
    value_heads = value_block.reshape(key_count, head_count, -1)
    scale = key_heads.shape[2] ** (-0.5)
    scores = (
        jnp.einsum("qhd,khd->hqk", query_heads, key_heads, preferred_element_type=jnp.float32)
        * scale
    )
    scores = scores + bias_block.astype(jnp.float32)[:, None, :]
    key_pos = key_start + lax.iota(jnp.int32, key_count)
    strict = ((key_pos[None, :] < query_pos[:, None]) & (key_pos[None, :] >= 0))[None]
    log_retained = jnp.where(strict, jax.nn.log_sigmoid(-scores), 0.0)
    between = lax.cumsum(log_retained, axis=2, reverse=True) - log_retained + kept_log[:, :, None]
    stick = jnp.where(strict, jnp.exp(jax.nn.log_sigmoid(scores) + between), 0.0).astype(
        jnp.bfloat16
    )
    accum = accum + jnp.einsum(
        "hqk,khd->qhd", stick, value_heads, preferred_element_type=jnp.float32
    )
    return (accum, kept_log + jnp.sum(log_retained, axis=2))


def normalize(middle_wide, norm_gain):
    mean_square = jnp.mean(middle_wide * middle_wide, axis=1, keepdims=True)
    return (middle_wide * lax.rsqrt(mean_square + norm_eps) * norm_gain.astype(jnp.float32)).astype(
        jnp.bfloat16
    )


def body(
    queries,
    key_rows,
    value_rows,
    key_bias,
    residual,
    out_weight,
    norm_gain,
    gate_weight,
    up_weight,
    down_weight,
):
    seg_rows = queries.shape[0]
    head_count = key_bias.shape[0]
    head_width = queries.shape[1] // head_count
    sp_count = lax.axis_size("sp")
    token_place = lax.axis_index("sp")
    query_heads = queries.reshape(seg_rows, head_count, head_width)
    query_pos = token_place * seg_rows + lax.iota(jnp.int32, seg_rows)
    start_carry = (
        jnp.zeros((seg_rows, head_count, head_width), jnp.float32),
        jnp.zeros((head_count, seg_rows), jnp.float32),
    )
    carry = stick_block(
        start_carry, query_heads, key_rows, value_rows, key_bias, query_pos, token_place * seg_rows
    )

    def advance(hop_index, state):
        carry_now, blocks = state
        blocks = from_behind((blocks[0], blocks[1], blocks[2]), "sp", 1)

        def attend(current):
            return stick_block(
                current,
                query_heads,
                blocks[0],
                blocks[1],
                blocks[2],
                query_pos,
                (token_place - hop_index) * seg_rows,
            )

        carry_now = lax.cond(token_place >= hop_index, attend, lambda current: current, carry_now)
        return (carry_now, blocks)

    carry, passed_blocks = lax.fori_loop(
        1, sp_count, advance, (carry, (key_rows, value_rows, key_bias))
    )
    attended = carry[0].reshape(seg_rows, head_count * head_width).astype(jnp.bfloat16)
    own_rows = seg_rows // lax.axis_size("tp")
    own_start = lax.axis_index("tp") * own_rows
    mixed = lax.psum_scatter(
        jnp.dot(attended, out_weight, preferred_element_type=jnp.float32).astype(jnp.bfloat16),
        "tp",
        scatter_dimension=0,
        tiled=True,
    ).astype(jnp.float32)
    own_residual = lax.dynamic_slice_in_dim(residual, own_start, own_rows, 0)
    middle = (own_residual.astype(jnp.float32) + mixed).astype(jnp.bfloat16)
    middle_wide = middle.astype(jnp.float32)
    normed_all = lax.all_gather(normalize(middle_wide, norm_gain), "tp", axis=0, tiled=True)
    gate_pre = jnp.dot(
        normed_all,
        lax.all_gather(gate_weight, "sp", axis=0, tiled=True),
        preferred_element_type=jnp.float32,
    )
    up_pre = jnp.dot(
        normed_all,
        lax.all_gather(up_weight, "sp", axis=0, tiled=True),
        preferred_element_type=jnp.float32,
    )
    hidden = (jax.nn.silu(gate_pre) * up_pre).astype(jnp.bfloat16)
    down_terms = jnp.dot(
        hidden,
        lax.all_gather(down_weight, "sp", axis=1, tiled=True),
        preferred_element_type=jnp.float32,
    )
    down_sum = lax.psum_scatter(
        down_terms.astype(jnp.bfloat16), "tp", scatter_dimension=0, tiled=True
    ).astype(jnp.float32)
    own_out = (middle_wide + down_sum).astype(jnp.bfloat16)
    return lax.all_gather(own_out, "tp", axis=0, tiled=True)


def solution(mesh):
    in_specs = (
        P(("grp", "sp"), "tp"),
        P(("grp", "sp"), "tp"),
        P(("grp", "sp"), "tp"),
        P("tp", ("grp", "sp")),
        P(("grp", "sp"), None),
        P("tp", None),
        P(),
        P("sp", "tp"),
        P("sp", "tp"),
        P("tp", "sp"),
    )
    out_specs = P(("grp", "sp"), None)
    return jax.shard_map(body, mesh=mesh, in_specs=in_specs, out_specs=out_specs, check_vma=False)
```

profile of v0, /device:TPU:0, one launch (start us, length us, event | category | flops | bytes accessed | tf_op | source)
XLA Modules:
  0.0 288.5 jit_solution(2027559084728312409)
XLA Ops:
  7.4 0.7 copy.51
  8.1 0.9 copy.19
  9.0 0.9 copy.20
  9.9 0.9 copy.21
  10.7 0.1 compare_and_fusion.1
  10.8 0.2 fusion.33
  11.1 0.1 fusion.36
  11.2 2.2 reduce_window_sum.16
  13.4 0.3 convolution_bitcast_fusion.1
  13.7 38.2 %while.22 = (s32[]{:T(128)}, f32[128,2,64]{0,2,1:T(8,128)S(1)}, f32[2,128]{1,0:T(2,128)S(1)}, bf16[128,128]{0,1:T(8,128)(2,1)S(1)}, bf16[128,128]{0,1:T(8,128)(2...) while((s32[]{:T(128)}, f32[128,2,64]{0,2,1:T(8,128)S(1)}, ...), condition=%wide.region_7.8_spmd.clone, body=%wide.region_2.7_spmd.clone.sunk | while | flops 13992710 | bytes 1652875 | solution.py:92
  13.7 5.0 %collective-permute-start = (bf16[128,128]{0,1:T(8,128)(2,1)S(1)}, bf16[128,128]{0,1:T(8,128)(2,1)S(1)}, u32[]{:S(2)}, u32[]{:S(2)}) collective-permute-start(bf16[128,128]{0,1:T(8,128)(2,1)S(1)} %get-tuple-element.347), channel_id=1, source_target_pairs={{0,4},{4,8},{8,12},{1,5},{5,9},{9,13},{2,6},{6,10},{10,14},{3,7},{... | collective-permute-start | bytes 98312 | tf_op jit(solution)/shard_map/while/body/eval_jaxpr/ppermute | solution.py:12
  18.7 3.5 %collective-permute-start.2 = (bf16[128,128]{0,1:T(8,128)(2,1)S(1)}, bf16[128,128]{0,1:T(8,128)(2,1)S(1)}, u32[]{:S(2)}, u32[]{:S(2)}) collective-permute-start(bf16[128,128]{0,1:T(8,128)(2,1)S(1)} %get-tuple-element.348), channel_id=1, source_target_pairs={{0,4},{4,8},{8,12},{1,5},{5,9},{9,13},{2,6},{6,10},{10,14},{3,7},{... | collective-permute-start | bytes 98312 | tf_op jit(solution)/shard_map/while/body/eval_jaxpr/ppermute | solution.py:12
  22.2 3.5 %collective-permute-start.1 = (bf16[2,128]{1,0:T(2,128)(2,1)S(1)}, bf16[2,128]{1,0:T(2,128)(2,1)S(1)}, u32[]{:S(2)}, u32[]{:S(2)}) collective-permute-start(bf16[2,128]{1,0:T(2,128)(2,1)S(1)} %get-tuple-element.349), channel_id=1, source_target_pairs={{0,4},{4,8},{8,12},{1,5},{5,9},{9,13},{2,6},{6,10},{10,14},{3,7},{... | collective-permute-start | bytes 1544 | tf_op jit(solution)/shard_map/while/body/eval_jaxpr/ppermute | solution.py:12
  25.7 1.3 collective-permute-done.1
  27.0 0.0 collective-permute-done
  27.0 0.0 collective-permute-done.2
  27.0 7.2 %collective-permute-start = (bf16[128,128]{0,1:T(8,128)(2,1)S(1)}, bf16[128,128]{0,1:T(8,128)(2,1)S(1)}, u32[]{:S(2)}, u32[]{:S(2)}) collective-permute-start(bf16[128,128]{0,1:T(8,128)(2,1)S(1)} %get-tuple-element.347), channel_id=1, source_target_pairs={{0,4},{4,8},{8,12},{1,5},{5,9},{9,13},{2,6},{6,10},{10,14},{3,7},{... | collective-permute-start | bytes 98312 | tf_op jit(solution)/shard_map/while/body/eval_jaxpr/ppermute | solution.py:12
  34.3 1.9 collective-permute-start.2
  36.2 1.9 collective-permute-start.1
  38.2 1.3 collective-permute-done.1
  39.5 4.2 %collective-permute-start = (bf16[128,128]{0,1:T(8,128)(2,1)S(1)}, bf16[128,128]{0,1:T(8,128)(2,1)S(1)}, u32[]{:S(2)}, u32[]{:S(2)}) collective-permute-start(bf16[128,128]{0,1:T(8,128)(2,1)S(1)} %get-tuple-element.347), channel_id=1, source_target_pairs={{0,4},{4,8},{8,12},{1,5},{5,9},{9,13},{2,6},{6,10},{10,14},{3,7},{... | collective-permute-start | bytes 98312 | tf_op jit(solution)/shard_map/while/body/eval_jaxpr/ppermute | solution.py:12
  43.7 5.0 %collective-permute-start.2 = (bf16[128,128]{0,1:T(8,128)(2,1)S(1)}, bf16[128,128]{0,1:T(8,128)(2,1)S(1)}, u32[]{:S(2)}, u32[]{:S(2)}) collective-permute-start(bf16[128,128]{0,1:T(8,128)(2,1)S(1)} %get-tuple-element.348), channel_id=1, source_target_pairs={{0,4},{4,8},{8,12},{1,5},{5,9},{9,13},{2,6},{6,10},{10,14},{3,7},{... | collective-permute-start | bytes 98312 | tf_op jit(solution)/shard_map/while/body/eval_jaxpr/ppermute | solution.py:12
  48.7 1.9 collective-permute-start.1
  50.6 1.3 collective-permute-done.1
  52.0 0.0 copy-start.1
  52.0 1.1 convolution_convert_fusion.1
  53.1 0.0 reduce-scatter.3.cloned.1.call-update
  53.2 0.0 all-gather.4.cloned.1.call-start
  53.2 0.5 all-gather.4.cloned.1.call-update
  53.7 0.0 all-gather.6.cloned.1.call-start
  53.8 0.5 all-gather.6.cloned.1.call-update
  54.3 0.0 all-gather.8.cloned.1.call-start
  54.4 0.5 all-gather.8.cloned.1.call-update
  54.9 0.0 reduce-scatter.5.cloned.1.call-start
  55.0 21.9 %reduce-scatter.3.cloned.1.call-done = bf16[32,2048]{1,0:T(8,128)(2,1)} async-done(((bf16[128,2048]{1,0:T(8,128)(2,1)}), bf16[32,2048]{1,0:T(8,128)(2,1)}) %reduce-scatter.3.cloned.1.call-update) | async-done | bytes 131088 | tf_op jit(solution)/shard_map/reduce_scatter | solution.py:98
  76.9 1.1 fusion.21
  78.0 0.1 fusion.23
  78.1 6.6 %all_gather.15 = bf16[128,2048]{1,0:T(8,128)(2,1)S(1)} all-gather(bf16[32,2048]{1,0:T(8,128)(2,1)S(1)} %fusion.23), channel_id=1, replica_groups=mesh['grp'=2,'sp'=4,'tp'=4] {'tp'}, dimensions={0}, use_global_device_ids=true | all-gather | bytes 655360 | tf_op jit(solution)/shard_map/all_gather | solution.py:107
  84.7 35.7 %all-gather.4.cloned.1.call-done = bf16[2048,768]{1,0:T(8,128)(2,1)} async-done(((bf16[512,768]{1,0:T(8,128)(2,1)}), bf16[2048,768]{1,0:T(8,128)(2,1)}) %all-gather.4.cloned.1.call-update) | async-done | bytes 3145744 | tf_op jit(solution)/shard_map/all_gather | solution.py:110
  120.4 2.5 fusion.37
  122.9 60.9 %all-gather.6.cloned.1.call-done = bf16[2048,768]{1,0:T(8,128)(2,1)} async-done(((bf16[512,768]{1,0:T(8,128)(2,1)}), bf16[2048,768]{1,0:T(8,128)(2,1)}) %all-gather.6.cloned.1.call-update) | async-done | bytes 3145744 | tf_op jit(solution)/shard_map/all_gather | solution.py:115
  183.8 63.4 %all-gather.8.cloned.1.call-done = bf16[768,2048]{1,0:T(8,128)(2,1)} async-done(((bf16[768,512]{1,0:T(8,128)(2,1)}), bf16[768,2048]{1,0:T(8,128)(2,1)}) %all-gather.8.cloned.1.call-update) | async-done | bytes 3145744 | tf_op jit(solution)/shard_map/all_gather | solution.py:121
  247.3 4.9 %convolution_convert_fusion = bf16[128,2048]{1,0:T(8,128)(2,1)} fusion(bf16[768,2048]{1,0:T(8,128)(2,1)} %all-gather.8.cloned.1.call-done, bf16[128,2048]{1,0:T(8,128)(2,1)S(1)} %all_gather.15, bf16[2048,768]{1,0:T(8,128)(2,1)} %all-gather.6.cloned.1.call-done, f32[128,768]{1,0:T(8,128)S(1)} %fusion.37), kind=kOutput, calls=%fused_computation.22 | convolution fusion | flops 806158336 | bytes 7733248 | tf_op jit(solution)/shard_map/dot_general | solution.py:119
  252.2 0.0 reduce-scatter.5.cloned.1.call-update
  252.2 20.4 %reduce-scatter.5.cloned.1.call-done = bf16[32,2048]{1,0:T(8,128)(2,1)} async-done(((bf16[128,2048]{1,0:T(8,128)(2,1)}), bf16[32,2048]{1,0:T(8,128)(2,1)}) %reduce-scatter.5.cloned.1.call-update) | async-done | bytes 131088 | tf_op jit(solution)/shard_map/reduce_scatter | solution.py:124
  272.6 0.9 fusion.24
  273.6 6.6 %all_gather.19 = bf16[128,2048]{1,0:T(8,128)(2,1)S(1)} all-gather(bf16[32,2048]{1,0:T(8,128)(2,1)S(1)} %fusion.24), channel_id=1, replica_groups=mesh['grp'=2,'sp'=4,'tp'=4] {'tp'}, dimensions={0}, use_global_device_ids=true | all-gather | bytes 655360 | tf_op jit(solution)/shard_map/all_gather | solution.py:128
  280.2 0.8 copy.52
  (29 shorter events, 0.1 us)
Async XLA Ops:
  7.4 44.6 %copy-start = (bf16[128,2048]{1,0:T(8,128)(2,1)S(1)}, bf16[128,2048]{1,0:T(8,128)(2,1)}, u32[]{:S(2)}) copy-start(bf16[128,2048]{1,0:T(8,128)(2,1)} %param.19) | copy-start | bytes 1572868
  7.4 69.5 %reduce-scatter.3.cloned.1.call-start = ((), (), s32[]{:S(2)}) async-start(), calls=%async_computation.2 | async-start | bytes 655360 | tf_op jit(solution)/shard_map/reduce_scatter | solution.py:98
  13.7 13.2 %collective-permute-start = (bf16[128,128]{0,1:T(8,128)(2,1)S(1)}, bf16[128,128]{0,1:T(8,128)(2,1)S(1)}, u32[]{:S(2)}, u32[]{:S(2)}) collective-permute-start(bf16[128,128]{0,1:T(8,128)(2,1)S(1)} %get-tuple-element.347), channel_id=1, source_target_pairs={{0,4},{4,8},{8,12},{1,5},{5,9},{9,13},{2,6},{6,10},{10,14},{3,7},{... | collective-permute-start | bytes 98312 | tf_op jit(solution)/shard_map/while/body/eval_jaxpr/ppermute | solution.py:12
  18.7 8.3 %collective-permute-start.2 = (bf16[128,128]{0,1:T(8,128)(2,1)S(1)}, bf16[128,128]{0,1:T(8,128)(2,1)S(1)}, u32[]{:S(2)}, u32[]{:S(2)}) collective-permute-start(bf16[128,128]{0,1:T(8,128)(2,1)S(1)} %get-tuple-element.348), channel_id=1, source_target_pairs={{0,4},{4,8},{8,12},{1,5},{5,9},{9,13},{2,6},{6,10},{10,14},{3,7},{... | collective-permute-start | bytes 98312 | tf_op jit(solution)/shard_map/while/body/eval_jaxpr/ppermute | solution.py:12
  22.2 4.8 %collective-permute-start.1 = (bf16[2,128]{1,0:T(2,128)(2,1)S(1)}, bf16[2,128]{1,0:T(2,128)(2,1)S(1)}, u32[]{:S(2)}, u32[]{:S(2)}) collective-permute-start(bf16[2,128]{1,0:T(2,128)(2,1)S(1)} %get-tuple-element.349), channel_id=1, source_target_pairs={{0,4},{4,8},{8,12},{1,5},{5,9},{9,13},{2,6},{6,10},{10,14},{3,7},{... | collective-permute-start | bytes 1544 | tf_op jit(solution)/shard_map/while/body/eval_jaxpr/ppermute | solution.py:12
  27.0 12.4 %collective-permute-start = (bf16[128,128]{0,1:T(8,128)(2,1)S(1)}, bf16[128,128]{0,1:T(8,128)(2,1)S(1)}, u32[]{:S(2)}, u32[]{:S(2)}) collective-permute-start(bf16[128,128]{0,1:T(8,128)(2,1)S(1)} %get-tuple-element.347), channel_id=1, source_target_pairs={{0,4},{4,8},{8,12},{1,5},{5,9},{9,13},{2,6},{6,10},{10,14},{3,7},{... | collective-permute-start | bytes 98312 | tf_op jit(solution)/shard_map/while/body/eval_jaxpr/ppermute | solution.py:12
  34.3 5.1 %collective-permute-start.2 = (bf16[128,128]{0,1:T(8,128)(2,1)S(1)}, bf16[128,128]{0,1:T(8,128)(2,1)S(1)}, u32[]{:S(2)}, u32[]{:S(2)}) collective-permute-start(bf16[128,128]{0,1:T(8,128)(2,1)S(1)} %get-tuple-element.348), channel_id=1, source_target_pairs={{0,4},{4,8},{8,12},{1,5},{5,9},{9,13},{2,6},{6,10},{10,14},{3,7},{... | collective-permute-start | bytes 98312 | tf_op jit(solution)/shard_map/while/body/eval_jaxpr/ppermute | solution.py:12
  36.2 3.2 %collective-permute-start.1 = (bf16[2,128]{1,0:T(2,128)(2,1)S(1)}, bf16[2,128]{1,0:T(2,128)(2,1)S(1)}, u32[]{:S(2)}, u32[]{:S(2)}) collective-permute-start(bf16[2,128]{1,0:T(2,128)(2,1)S(1)} %get-tuple-element.349), channel_id=1, source_target_pairs={{0,4},{4,8},{8,12},{1,5},{5,9},{9,13},{2,6},{6,10},{10,14},{3,7},{... | collective-permute-start | bytes 1544 | tf_op jit(solution)/shard_map/while/body/eval_jaxpr/ppermute | solution.py:12
  39.5 12.4 %collective-permute-start = (bf16[128,128]{0,1:T(8,128)(2,1)S(1)}, bf16[128,128]{0,1:T(8,128)(2,1)S(1)}, u32[]{:S(2)}, u32[]{:S(2)}) collective-permute-start(bf16[128,128]{0,1:T(8,128)(2,1)S(1)} %get-tuple-element.347), channel_id=1, source_target_pairs={{0,4},{4,8},{8,12},{1,5},{5,9},{9,13},{2,6},{6,10},{10,14},{3,7},{... | collective-permute-start | bytes 98312 | tf_op jit(solution)/shard_map/while/body/eval_jaxpr/ppermute | solution.py:12
  43.7 8.2 %collective-permute-start.2 = (bf16[128,128]{0,1:T(8,128)(2,1)S(1)}, bf16[128,128]{0,1:T(8,128)(2,1)S(1)}, u32[]{:S(2)}, u32[]{:S(2)}) collective-permute-start(bf16[128,128]{0,1:T(8,128)(2,1)S(1)} %get-tuple-element.348), channel_id=1, source_target_pairs={{0,4},{4,8},{8,12},{1,5},{5,9},{9,13},{2,6},{6,10},{10,14},{3,7},{... | collective-permute-start | bytes 98312 | tf_op jit(solution)/shard_map/while/body/eval_jaxpr/ppermute | solution.py:12
  48.7 3.2 %collective-permute-start.1 = (bf16[2,128]{1,0:T(2,128)(2,1)S(1)}, bf16[2,128]{1,0:T(2,128)(2,1)S(1)}, u32[]{:S(2)}, u32[]{:S(2)}) collective-permute-start(bf16[2,128]{1,0:T(2,128)(2,1)S(1)} %get-tuple-element.349), channel_id=1, source_target_pairs={{0,4},{4,8},{8,12},{1,5},{5,9},{9,13},{2,6},{6,10},{10,14},{3,7},{... | collective-permute-start | bytes 1544 | tf_op jit(solution)/shard_map/while/body/eval_jaxpr/ppermute | solution.py:12
  52.0 3.0 %copy-start.1 = (bf16[2048]{0:T(1024)(128)(2,1)S(1)}, bf16[2048]{0:T(1024)(128)(2,1)}, u32[]{:S(2)}) copy-start(bf16[2048]{0:T(1024)(128)(2,1)} %param.20) | copy-start | bytes 12292
  53.2 67.3 %all-gather.4.cloned.1.call-start = ((), (), s32[]{:S(2)}) async-start(), calls=%async_computation.3 | async-start | bytes 3932160 | tf_op jit(solution)/shard_map/all_gather | solution.py:110
  53.7 130.1 %all-gather.6.cloned.1.call-start = ((), (), s32[]{:S(2)}) async-start(), calls=%async_computation.4 | async-start | bytes 3932160 | tf_op jit(solution)/shard_map/all_gather | solution.py:115
  54.3 192.9 %all-gather.8.cloned.1.call-start = ((), (), s32[]{:S(2)}) async-start(), calls=%async_computation.5 | async-start | bytes 3932160 | tf_op jit(solution)/shard_map/all_gather | solution.py:121
  54.9 217.7 %reduce-scatter.5.cloned.1.call-start = ((), (), s32[]{:S(2)}) async-start(), calls=%async_computation.6 | async-start | bytes 655360 | tf_op jit(solution)/shard_map/reduce_scatter | solution.py:124
Sparse Core Ops, SparseCore 0:
  53.3 23.5 reduce-scatter.2
  252.3 20.2 reduce-scatter.4
Sparse Core Ops, SparseCore 1:
  55.2 65.2 all-gather.3
  121.9 61.9 all-gather.5
  185.3 61.9 all-gather.7
where the time goes:
time: 289 us
  waiting for transfers between devices  208 us (72%)
  starting transfers between devices  34.3 us (12%)
  between operations  15.1 us (5%)
  blocking collectives  13.2 us (5%)
  matrix products  9.04 us (3%)
  other arithmetic  4.64 us (2%)
  local copies, waits for them, and re-layouts  4.15 us (1%)
    all_gather x1, waiting for transfers between devices, body(): lax.all_gather(down_weight, 'sp', axis=1, tiled=True)  63.4 us
    all_gather x1, waiting for transfers between devices, body(): lax.all_gather(up_weight, 'sp', axis=0, tiled=True)  60.9 us
    all_gather x1, waiting for transfers between devices, body(): lax.all_gather(gate_weight, 'sp', axis=0, tiled=True)  35.7 us
    ppermute x9, starting transfers between devices, from_behind(): lax.ppermute(value, axis, [(source, source + steps) for source in range(i...  34.1 us
    reduce_scatter x1, waiting for transfers between devices, body(): lax.psum_scatter(jnp.dot(attended, out_weight, preferred_element_type=jnp...  21.9 us
    reduce_scatter x1, waiting for transfers between devices, body(): lax.psum_scatter(down_terms.astype(jnp.bfloat16), 'tp', scatter_dimension...  20.4 us
    all_gather x1, blocking collectives, body(): lax.all_gather(normalize(middle_wide, norm_gain), 'tp', axis=0, tiled=True)  6.6 us
    all_gather x1, blocking collectives, body(): return lax.all_gather(own_out, 'tp', axis=0, tiled=True)  6.58 us
  transfers between devices with their start and end apart: 14, of which 8 were waited for; matrix products, arithmetic and copies ran while one was open for 1% of the time, Pallas kernels for 0%

commit v1 on v0

--- a/solution.py
+++ b/solution.py
@@ -118,7 +118,7 @@
     hidden = (jax.nn.silu(gate_pre) * up_pre).astype(jnp.bfloat16)
     down_terms = jnp.dot(
         hidden,
-        lax.all_gather(down_weight, "sp", axis=1, tiled=True),
+        jnp.concatenate(lax.all_gather(down_weight, "sp"), axis=1),
         preferred_element_type=jnp.float32,
     )
     down_sum = lax.psum_scatter(

time: 289 us -> 290 us (level)
  waiting for transfers between devices: 208 us -> 203 us
  local copies, waits for them, and re-layouts: 4.15 us -> 8.8 us
    all_gather x1, waiting for transfers between devices: 63.4 us -> 35.7 us  [body(): lax.all_gather(down_weight, 'sp')]
    all_gather x1, waiting for transfers between devices: 35.7 us -> 58.8 us  [body(): lax.all_gather(gate_weight, 'sp', axis=0, tiled=True)]
    reshape x0 -> x1, local copies, waits for them, and re-layouts: none -> 4.65 us  [body(): jnp.concatenate(lax.all_gather(down_weight, 'sp'), axis=1)]
  transfers between devices with their start and end apart: 14 -> 14, of which waited for: 8 -> 8; matrix products, arithmetic and copies ran while one was open for 1% -> 3% of each run, Pallas kernels for 0% -> 0%
where the time goes in v1:
time: 290 us; the launch traced here: 289 us
  waiting for transfers between devices  203 us (70%)
  starting transfers between devices  34.3 us (12%)
  between operations  15.1 us (5%)
  blocking collectives  13.2 us (5%)
  matrix products  9.43 us (3%)
  local copies, waits for them, and re-layouts  8.8 us (3%)
  other arithmetic  4.64 us (2%)
    all_gather x1, waiting for transfers between devices, body(): lax.all_gather(up_weight, 'sp', axis=0, tiled=True)  60.9 us
    all_gather x1, waiting for transfers between devices, body(): lax.all_gather(gate_weight, 'sp', axis=0, tiled=True)  58.8 us
    all_gather x1, waiting for transfers between devices, body(): lax.all_gather(down_weight, 'sp')  35.7 us
    ppermute x9, starting transfers between devices, from_behind(): lax.ppermute(value, axis, [(source, source + steps) for source in range(i...  34.1 us
    reduce_scatter x1, waiting for transfers between devices, body(): lax.psum_scatter(jnp.dot(attended, out_weight, preferred_element_type=jnp...  21.9 us
    reduce_scatter x1, waiting for transfers between devices, body(): lax.psum_scatter(down_terms.astype(jnp.bfloat16), 'tp', scatter_dimension...  20.4 us
    all_gather x1, blocking collectives, body(): lax.all_gather(normalize(middle_wide, norm_gain), 'tp', axis=0, tiled=True)  6.6 us
    all_gather x1, blocking collectives, body(): return lax.all_gather(own_out, 'tp', axis=0, tiled=True)  6.58 us
  transfers between devices with their start and end apart: 14, of which 8 were waited for; matrix products, arithmetic and copies ran while one was open for 3% of the time, Pallas kernels for 0%

profile of v1, /device:TPU:0, one launch (start us, length us, event | category | flops | bytes accessed | tf_op | source)
XLA Modules:
  0.0 288.9 jit_solution(6189614997878790938)
XLA Ops:
  7.4 0.7 copy.59
  8.1 0.9 copy.26
  9.0 0.9 copy.27
  9.9 0.9 copy.28
  10.7 0.1 compare_and_fusion.1
  10.8 0.2 fusion.33
  11.1 0.1 fusion.36
  11.2 2.2 reduce_window_sum.16
  13.4 0.3 convolution_bitcast_fusion.1
  13.7 38.2 %while.22 = (s32[]{:T(128)}, f32[128,2,64]{0,2,1:T(8,128)S(1)}, f32[2,128]{1,0:T(2,128)S(1)}, bf16[128,128]{0,1:T(8,128)(2,1)S(1)}, bf16[128,128]{0,1:T(8,128)(2...) while((s32[]{:T(128)}, f32[128,2,64]{0,2,1:T(8,128)S(1)}, ...), condition=%wide.region_7.8_spmd.clone, body=%wide.region_2.7_spmd.clone.sunk | while | flops 13992710 | bytes 1652875 | solution.py:92
  13.7 5.0 %collective-permute-start = (bf16[128,128]{0,1:T(8,128)(2,1)S(1)}, bf16[128,128]{0,1:T(8,128)(2,1)S(1)}, u32[]{:S(2)}, u32[]{:S(2)}) collective-permute-start(bf16[128,128]{0,1:T(8,128)(2,1)S(1)} %get-tuple-element.356), channel_id=1, source_target_pairs={{0,4},{4,8},{8,12},{1,5},{5,9},{9,13},{2,6},{6,10},{10,14},{3,7},{... | collective-permute-start | bytes 98312 | tf_op jit(solution)/shard_map/while/body/eval_jaxpr/ppermute | solution.py:12
  18.7 3.5 %collective-permute-start.2 = (bf16[128,128]{0,1:T(8,128)(2,1)S(1)}, bf16[128,128]{0,1:T(8,128)(2,1)S(1)}, u32[]{:S(2)}, u32[]{:S(2)}) collective-permute-start(bf16[128,128]{0,1:T(8,128)(2,1)S(1)} %get-tuple-element.357), channel_id=1, source_target_pairs={{0,4},{4,8},{8,12},{1,5},{5,9},{9,13},{2,6},{6,10},{10,14},{3,7},{... | collective-permute-start | bytes 98312 | tf_op jit(solution)/shard_map/while/body/eval_jaxpr/ppermute | solution.py:12
  22.2 3.5 %collective-permute-start.1 = (bf16[2,128]{1,0:T(2,128)(2,1)S(1)}, bf16[2,128]{1,0:T(2,128)(2,1)S(1)}, u32[]{:S(2)}, u32[]{:S(2)}) collective-permute-start(bf16[2,128]{1,0:T(2,128)(2,1)S(1)} %get-tuple-element.358), channel_id=1, source_target_pairs={{0,4},{4,8},{8,12},{1,5},{5,9},{9,13},{2,6},{6,10},{10,14},{3,7},{... | collective-permute-start | bytes 1544 | tf_op jit(solution)/shard_map/while/body/eval_jaxpr/ppermute | solution.py:12
  25.7 1.3 collective-permute-done.1
  27.0 7.2 %collective-permute-start = (bf16[128,128]{0,1:T(8,128)(2,1)S(1)}, bf16[128,128]{0,1:T(8,128)(2,1)S(1)}, u32[]{:S(2)}, u32[]{:S(2)}) collective-permute-start(bf16[128,128]{0,1:T(8,128)(2,1)S(1)} %get-tuple-element.356), channel_id=1, source_target_pairs={{0,4},{4,8},{8,12},{1,5},{5,9},{9,13},{2,6},{6,10},{10,14},{3,7},{... | collective-permute-start | bytes 98312 | tf_op jit(solution)/shard_map/while/body/eval_jaxpr/ppermute | solution.py:12
  34.3 1.9 collective-permute-start.2
  36.2 1.9 collective-permute-start.1
  38.2 1.3 collective-permute-done.1
  39.4 0.0 collective-permute-done
  39.5 4.2 %collective-permute-start = (bf16[128,128]{0,1:T(8,128)(2,1)S(1)}, bf16[128,128]{0,1:T(8,128)(2,1)S(1)}, u32[]{:S(2)}, u32[]{:S(2)}) collective-permute-start(bf16[128,128]{0,1:T(8,128)(2,1)S(1)} %get-tuple-element.356), channel_id=1, source_target_pairs={{0,4},{4,8},{8,12},{1,5},{5,9},{9,13},{2,6},{6,10},{10,14},{3,7},{... | collective-permute-start | bytes 98312 | tf_op jit(solution)/shard_map/while/body/eval_jaxpr/ppermute | solution.py:12
  43.7 5.0 %collective-permute-start.2 = (bf16[128,128]{0,1:T(8,128)(2,1)S(1)}, bf16[128,128]{0,1:T(8,128)(2,1)S(1)}, u32[]{:S(2)}, u32[]{:S(2)}) collective-permute-start(bf16[128,128]{0,1:T(8,128)(2,1)S(1)} %get-tuple-element.357), channel_id=1, source_target_pairs={{0,4},{4,8},{8,12},{1,5},{5,9},{9,13},{2,6},{6,10},{10,14},{3,7},{... | collective-permute-start | bytes 98312 | tf_op jit(solution)/shard_map/while/body/eval_jaxpr/ppermute | solution.py:12
  48.7 1.9 collective-permute-start.1
  50.6 1.3 collective-permute-done.1
  52.0 0.0 copy-start.1
  52.0 1.1 convolution_convert_fusion.1
  53.1 0.0 reduce-scatter.3.cloned.1.call-update
  53.2 0.0 all-gather.9.cloned.1.call-start
  53.2 0.5 all-gather.9.cloned.1.call-update
  53.7 0.0 all-gather.5.cloned.1.call-start
  53.8 0.5 all-gather.5.cloned.1.call-update
  54.3 0.0 all-gather.7.cloned.1.call-start
  54.4 0.5 all-gather.7.cloned.1.call-update
  54.9 0.0 reduce-scatter.5.cloned.1.call-start
  55.0 21.9 %reduce-scatter.3.cloned.1.call-done = bf16[32,2048]{1,0:T(8,128)(2,1)} async-done(((bf16[128,2048]{1,0:T(8,128)(2,1)}), bf16[32,2048]{1,0:T(8,128)(2,1)}) %reduce-scatter.3.cloned.1.call-update) | async-done | bytes 131088 | tf_op jit(solution)/shard_map/reduce_scatter | solution.py:98
  76.9 1.1 fusion.21
  78.0 0.1 fusion.23
  78.1 6.6 %all_gather.18 = bf16[128,2048]{1,0:T(8,128)(2,1)S(1)} all-gather(bf16[32,2048]{1,0:T(8,128)(2,1)S(1)} %fusion.23), channel_id=1, replica_groups=mesh['grp'=2,'sp'=4,'tp'=4] {'tp'}, dimensions={0}, use_global_device_ids=true | all-gather | bytes 655360 | tf_op jit(solution)/shard_map/all_gather | solution.py:107
  84.7 35.7 %all-gather.9.cloned.1.call-done = bf16[3072,512]{1,0:T(8,128)(2,1)} async-done(((bf16[768,512]{1,0:T(8,128)(2,1)}), bf16[3072,512]{1,0:T(8,128)(2,1)}) %all-gather.9.cloned.1.call-update) | async-done | bytes 3145744 | tf_op jit(solution)/shard_map/all_gather | solution.py:121
  120.4 4.7 %copy.32 = bf16[768,4,512]{0,2,1:T(8,128)(2,1)} copy(bf16[768,4,512]{2,0,1:T(8,128)(2,1)} %bitcast.30) | data formatting | bytes 6291456 | tf_op jit(solution)/shard_map/reshape | solution.py:121
  125.1 58.8 %all-gather.5.cloned.1.call-done = bf16[2048,768]{1,0:T(8,128)(2,1)} async-done(((bf16[512,768]{1,0:T(8,128)(2,1)}), bf16[2048,768]{1,0:T(8,128)(2,1)}) %all-gather.5.cloned.1.call-update) | async-done | bytes 3145744 | tf_op jit(solution)/shard_map/all_gather | solution.py:110
  183.8 2.5 fusion.37
  186.3 60.9 %all-gather.7.cloned.1.call-done = bf16[2048,768]{1,0:T(8,128)(2,1)} async-done(((bf16[512,768]{1,0:T(8,128)(2,1)}), bf16[2048,768]{1,0:T(8,128)(2,1)}) %all-gather.7.cloned.1.call-update) | async-done | bytes 3145744 | tf_op jit(solution)/shard_map/all_gather | solution.py:115
  247.3 5.3 %convolution_convert_fusion = bf16[128,2048]{1,0:T(8,128)(2,1)} fusion(bf16[768,2048]{0,1:T(8,128)(2,1)} %bitcast.31, bf16[128,2048]{1,0:T(8,128)(2,1)S(1)} %all_gather.18, bf16[2048,768]{1,0:T(8,128)(2,1)} %all-gather.7.cloned.1.call-done, f32[128,768]{1,0:T(8,128)S(1)} %fusion.37), kind=kOutput, calls=%fused_computation.22 | convolution fusion | flops 806158336 | bytes 7733248 | tf_op jit(solution)/shard_map/dot_general | solution.py:119
  252.6 0.0 reduce-scatter.5.cloned.1.call-update
  252.6 20.4 %reduce-scatter.5.cloned.1.call-done = bf16[32,2048]{1,0:T(8,128)(2,1)} async-done(((bf16[128,2048]{1,0:T(8,128)(2,1)}), bf16[32,2048]{1,0:T(8,128)(2,1)}) %reduce-scatter.5.cloned.1.call-update) | async-done | bytes 131088 | tf_op jit(solution)/shard_map/reduce_scatter | solution.py:124
  273.0 0.9 fusion.24
  274.0 6.6 %all_gather.23 = bf16[128,2048]{1,0:T(8,128)(2,1)S(1)} all-gather(bf16[32,2048]{1,0:T(8,128)(2,1)S(1)} %fusion.24), channel_id=1, replica_groups=mesh['grp'=2,'sp'=4,'tp'=4] {'tp'}, dimensions={0}, use_global_device_ids=true | all-gather | bytes 655360 | tf_op jit(solution)/shard_map/all_gather | solution.py:128
  280.5 0.8 copy.60
  (30 shorter events, 0.1 us)
Async XLA Ops:
  7.4 44.6 %copy-start = (bf16[128,2048]{1,0:T(8,128)(2,1)S(1)}, bf16[128,2048]{1,0:T(8,128)(2,1)}, u32[]{:S(2)}) copy-start(bf16[128,2048]{1,0:T(8,128)(2,1)} %param.19) | copy-start | bytes 1572868
  7.4 69.5 %reduce-scatter.3.cloned.1.call-start = ((), (), s32[]{:S(2)}) async-start(), calls=%async_computation.2 | async-start | bytes 655360 | tf_op jit(solution)/shard_map/reduce_scatter | solution.py:98
  13.7 13.2 %collective-permute-start = (bf16[128,128]{0,1:T(8,128)(2,1)S(1)}, bf16[128,128]{0,1:T(8,128)(2,1)S(1)}, u32[]{:S(2)}, u32[]{:S(2)}) collective-permute-start(bf16[128,128]{0,1:T(8,128)(2,1)S(1)} %get-tuple-element.356), channel_id=1, source_target_pairs={{0,4},{4,8},{8,12},{1,5},{5,9},{9,13},{2,6},{6,10},{10,14},{3,7},{... | collective-permute-start | bytes 98312 | tf_op jit(solution)/shard_map/while/body/eval_jaxpr/ppermute | solution.py:12
  18.7 8.3 %collective-permute-start.2 = (bf16[128,128]{0,1:T(8,128)(2,1)S(1)}, bf16[128,128]{0,1:T(8,128)(2,1)S(1)}, u32[]{:S(2)}, u32[]{:S(2)}) collective-permute-start(bf16[128,128]{0,1:T(8,128)(2,1)S(1)} %get-tuple-element.357), channel_id=1, source_target_pairs={{0,4},{4,8},{8,12},{1,5},{5,9},{9,13},{2,6},{6,10},{10,14},{3,7},{... | collective-permute-start | bytes 98312 | tf_op jit(solution)/shard_map/while/body/eval_jaxpr/ppermute | solution.py:12
  22.2 4.8 %collective-permute-start.1 = (bf16[2,128]{1,0:T(2,128)(2,1)S(1)}, bf16[2,128]{1,0:T(2,128)(2,1)S(1)}, u32[]{:S(2)}, u32[]{:S(2)}) collective-permute-start(bf16[2,128]{1,0:T(2,128)(2,1)S(1)} %get-tuple-element.358), channel_id=1, source_target_pairs={{0,4},{4,8},{8,12},{1,5},{5,9},{9,13},{2,6},{6,10},{10,14},{3,7},{... | collective-permute-start | bytes 1544 | tf_op jit(solution)/shard_map/while/body/eval_jaxpr/ppermute | solution.py:12
  27.0 12.4 %collective-permute-start = (bf16[128,128]{0,1:T(8,128)(2,1)S(1)}, bf16[128,128]{0,1:T(8,128)(2,1)S(1)}, u32[]{:S(2)}, u32[]{:S(2)}) collective-permute-start(bf16[128,128]{0,1:T(8,128)(2,1)S(1)} %get-tuple-element.356), channel_id=1, source_target_pairs={{0,4},{4,8},{8,12},{1,5},{5,9},{9,13},{2,6},{6,10},{10,14},{3,7},{... | collective-permute-start | bytes 98312 | tf_op jit(solution)/shard_map/while/body/eval_jaxpr/ppermute | solution.py:12
  34.3 5.1 %collective-permute-start.2 = (bf16[128,128]{0,1:T(8,128)(2,1)S(1)}, bf16[128,128]{0,1:T(8,128)(2,1)S(1)}, u32[]{:S(2)}, u32[]{:S(2)}) collective-permute-start(bf16[128,128]{0,1:T(8,128)(2,1)S(1)} %get-tuple-element.357), channel_id=1, source_target_pairs={{0,4},{4,8},{8,12},{1,5},{5,9},{9,13},{2,6},{6,10},{10,14},{3,7},{... | collective-permute-start | bytes 98312 | tf_op jit(solution)/shard_map/while/body/eval_jaxpr/ppermute | solution.py:12
  36.2 3.2 %collective-permute-start.1 = (bf16[2,128]{1,0:T(2,128)(2,1)S(1)}, bf16[2,128]{1,0:T(2,128)(2,1)S(1)}, u32[]{:S(2)}, u32[]{:S(2)}) collective-permute-start(bf16[2,128]{1,0:T(2,128)(2,1)S(1)} %get-tuple-element.358), channel_id=1, source_target_pairs={{0,4},{4,8},{8,12},{1,5},{5,9},{9,13},{2,6},{6,10},{10,14},{3,7},{... | collective-permute-start | bytes 1544 | tf_op jit(solution)/shard_map/while/body/eval_jaxpr/ppermute | solution.py:12
  39.5 12.4 %collective-permute-start = (bf16[128,128]{0,1:T(8,128)(2,1)S(1)}, bf16[128,128]{0,1:T(8,128)(2,1)S(1)}, u32[]{:S(2)}, u32[]{:S(2)}) collective-permute-start(bf16[128,128]{0,1:T(8,128)(2,1)S(1)} %get-tuple-element.356), channel_id=1, source_target_pairs={{0,4},{4,8},{8,12},{1,5},{5,9},{9,13},{2,6},{6,10},{10,14},{3,7},{... | collective-permute-start | bytes 98312 | tf_op jit(solution)/shard_map/while/body/eval_jaxpr/ppermute | solution.py:12
  43.7 8.2 %collective-permute-start.2 = (bf16[128,128]{0,1:T(8,128)(2,1)S(1)}, bf16[128,128]{0,1:T(8,128)(2,1)S(1)}, u32[]{:S(2)}, u32[]{:S(2)}) collective-permute-start(bf16[128,128]{0,1:T(8,128)(2,1)S(1)} %get-tuple-element.357), channel_id=1, source_target_pairs={{0,4},{4,8},{8,12},{1,5},{5,9},{9,13},{2,6},{6,10},{10,14},{3,7},{... | collective-permute-start | bytes 98312 | tf_op jit(solution)/shard_map/while/body/eval_jaxpr/ppermute | solution.py:12
  48.7 3.2 %collective-permute-start.1 = (bf16[2,128]{1,0:T(2,128)(2,1)S(1)}, bf16[2,128]{1,0:T(2,128)(2,1)S(1)}, u32[]{:S(2)}, u32[]{:S(2)}) collective-permute-start(bf16[2,128]{1,0:T(2,128)(2,1)S(1)} %get-tuple-element.358), channel_id=1, source_target_pairs={{0,4},{4,8},{8,12},{1,5},{5,9},{9,13},{2,6},{6,10},{10,14},{3,7},{... | collective-permute-start | bytes 1544 | tf_op jit(solution)/shard_map/while/body/eval_jaxpr/ppermute | solution.py:12
  52.0 3.0 %copy-start.1 = (bf16[2048]{0:T(1024)(128)(2,1)S(1)}, bf16[2048]{0:T(1024)(128)(2,1)}, u32[]{:S(2)}) copy-start(bf16[2048]{0:T(1024)(128)(2,1)} %param.20) | copy-start | bytes 12292
  53.2 67.3 %all-gather.9.cloned.1.call-start = ((), (), s32[]{:S(2)}) async-start(), calls=%async_computation.6 | async-start | bytes 3932160 | tf_op jit(solution)/shard_map/all_gather | solution.py:121
  53.7 130.1 %all-gather.5.cloned.1.call-start = ((), (), s32[]{:S(2)}) async-start(), calls=%async_computation.3 | async-start | bytes 3932160 | tf_op jit(solution)/shard_map/all_gather | solution.py:110
  54.3 192.9 %all-gather.7.cloned.1.call-start = ((), (), s32[]{:S(2)}) async-start(), calls=%async_computation.4 | async-start | bytes 3932160 | tf_op jit(solution)/shard_map/all_gather | solution.py:115
  54.9 218.1 %reduce-scatter.5.cloned.1.call-start = ((), (), s32[]{:S(2)}) async-start(), calls=%async_computation.5 | async-start | bytes 655360 | tf_op jit(solution)/shard_map/reduce_scatter | solution.py:124
Sparse Core Ops, SparseCore 0:
  53.3 23.5 reduce-scatter.2
  252.7 20.2 reduce-scatter.4
Sparse Core Ops, SparseCore 1:
  55.2 65.2 all-gather.8
  121.9 61.9 all-gather.4
  185.3 61.9 all-gather.6
